TPU v7x, 256 devices: a whole 4x4x8 slice. The times are simulated.
256 devices in a mesh: kv: 32 (over z, y), tp: 8 (over x, core).
Axes of the slice: x: 4, y: 4, z: 8, core: 2. Of those that a mesh axis runs over, the one named last changes fastest.
Arguments:
- stream: bfloat16 [128, 4096], P(None, ('kv', 'tp')), may hold values from -60 to 60
- memory_state: float32 [128, 32, 128, 128], P('kv', 'tp'), may hold values from -3 to 3
- attn_gain: float32 [4096], P('kv'), may hold values from 0.1 to 1.9
- query_weight: bfloat16 [4096, 4096], P('kv', 'tp'), may hold values from -0.09375 to 0.09375
- key_weight: bfloat16 [4096, 4096], P('kv', 'tp'), may hold values from -0.09375 to 0.09375
- value_weight: bfloat16 [4096, 4096], P('kv', 'tp'), may hold values from -0.09375 to 0.09375
- outgate_weight: bfloat16 [4096, 4096], P('kv', 'tp'), may hold values from -0.09375 to 0.09375
- beta_weight: bfloat16 [4096, 32], P('kv', 'tp'), may hold values from -0.09375 to 0.09375
- decay_weight: bfloat16 [4096, 32], P('kv', 'tp'), may hold values from -0.09375 to 0.09375
- decay_log: float32 [32], P('tp'), may hold values from -4 to 1
- decay_shift: float32 [32], P('tp'), may hold values from -3 to 3
- head_gain: float32 [128], replicated, may hold values from 0.1 to 1.9
- output_weight: bfloat16 [4096, 4096], P('tp', 'kv'), may hold values from -0.09375 to 0.09375
- mixer_gain: float32 [4096], P('kv'), may hold values from 0.1 to 1.9
- up_weight: bfloat16 [4096, 16384], P('kv', 'tp'), may hold values from -0.09375 to 0.09375
- down_weight: bfloat16 [16384, 4096], P('tp', 'kv'), may hold values from -0.046875 to 0.046875
Outputs:
- layer_out: bfloat16 [128, 4096], P(None, ('kv', 'tp'))
- memory_next: float32 [128, 32, 128, 128], P('kv', 'tp')
All inputs are finite; a program needn't handle non-finite values.
Results may differ from a plain program's by a relative error of at most 0.025.
Values may be sent and summed in bfloat16 or wider, within the bound.
A program may use at most 64 MiB of HBM per device.

v0:
```python
import jax
import jax.numpy as jnp
from jax import lax
from jax.sharding import PartitionSpec as P

D = 4096
HEAD_DIM = 128
epsilon = 1e-06


def split_up(value, dim, length):
    dims = value.shape
    pieces = value.reshape(*dims[:dim], length, dims[dim] // length, *dims[dim + 1 :])
    return jnp.moveaxis(pieces, dim, 0)


def sent_and_summed(value, axis, dim):
    length = lax.axis_size(axis)
    pieces = lax.all_to_all(split_up(value, dim, length), axis, 0, 0, tiled=True)
    return jnp.sum(pieces.astype(jnp.float32), axis=0)


def side_by_side(arrays, axis, dim, along):
    columns = [a.reshape(*a.shape[:along], -1) for a in arrays]
    both = jnp.concatenate(columns, axis=along)
    out, at, gathered = (sent_and_summed(both, axis, dim), 0, [])
    for a, column in zip(arrays, columns):
        share = out[..., at : at + column.shape[along]]
        gathered.append(share.reshape(*share.shape[:along], *a.shape[along:]))
        at += column.shape[along]
    return tuple(gathered)


def joined_along(pieces, dim):
    dims = list(pieces.shape[1:])
    dims[dim] *= pieces.shape[0]
    return jnp.moveaxis(pieces, 0, dim).reshape(dims)


def copy_for_each(value, axis):
    copies = jnp.broadcast_to(value, (lax.axis_size(axis), *value.shape))
    return lax.all_to_all(copies, axis, split_axis=0, concat_axis=0, tiled=True)


def collect(value, axis, dim):
    return joined_along(copy_for_each(value, axis), dim)


def sent_and_summed_2(value, axis, dim):
    pieces = split_up(value, dim, lax.axis_size(axis))
    arrived = lax.all_to_all(pieces, axis, split_axis=0, concat_axis=0, tiled=True)
    return arrived.sum(axis=0)


def gathered_rows(stream, gain_vec):
    gathered = lax.all_gather(stream, "tp", axis=1, tiled=True)
    widened = gathered.astype(jnp.float32)
    squares = jnp.sum(widened * widened, axis=1)
    scaled = (widened * gain_vec).astype(jnp.bfloat16)
    return (scaled, squares)


def unit_rows(values):
    return values * lax.rsqrt(jnp.sum(values * values, axis=-1, keepdims=True) + epsilon)


def head_output(
    memory_state,
    query_sum,
    key_sum,
    value_sum,
    gate_sum,
    beta_sum,
    decay_sum,
    decay_log,
    decay_shift,
    head_gain,
):
    row_count = query_sum.shape[0]
    head_count = beta_sum.shape[1]

    def to_heads(values):
        return values.reshape(row_count, head_count, HEAD_DIM)

    query_heads = unit_rows(jax.nn.silu(to_heads(query_sum))) * HEAD_DIM ** (-0.5)
    key_heads = unit_rows(jax.nn.silu(to_heads(key_sum)))
    value_heads = jax.nn.silu(to_heads(value_sum))
    beta_heads = jax.nn.sigmoid(beta_sum)
    decay_heads = jnp.exp(-jnp.exp(decay_log) * jax.nn.softplus(decay_sum + decay_shift))
    kept_state = memory_state * decay_heads[:, :, None, None]
    recalled = jnp.einsum("bhkv,bhk->bhv", kept_state, key_heads)
    correction = beta_heads[:, :, None] * (value_heads - recalled)
    memory_next = kept_state + key_heads[:, :, :, None] * correction[:, :, None, :]
    readout = jnp.einsum("bhkv,bhk->bhv", memory_next, query_heads)
    normed = readout * lax.rsqrt(jnp.mean(readout * readout, axis=-1, keepdims=True) + epsilon)
    gated = normed * head_gain * jax.nn.silu(to_heads(gate_sum))
    return (gated.reshape(row_count, head_count * HEAD_DIM).astype(jnp.bfloat16), memory_next)


def shards(
    stream,
    memory_state,
    attn_gain,
    query_weight,
    key_weight,
    value_weight,
    outgate_weight,
    beta_weight,
    decay_weight,
    decay_log,
    decay_shift,
    head_gain,
    output_weight,
    mixer_gain,
    up_weight,
    down_weight,
):
    scaled, squares = gathered_rows(stream, attn_gain)

    def product(weight):
        return jnp.dot(scaled, weight, preferred_element_type=jnp.float32)

    query_sum, key_sum, value_sum, gate_sum, beta_sum, decay_sum, own_squares = side_by_side(
        (
            product(query_weight).astype(jnp.bfloat16),
            product(key_weight).astype(jnp.bfloat16),
            product(value_weight).astype(jnp.bfloat16),
            product(outgate_weight).astype(jnp.bfloat16),
            product(beta_weight).astype(jnp.bfloat16),
            product(decay_weight).astype(jnp.bfloat16),
            squares.astype(jnp.bfloat16),
        ),
        "kv",
        0,
        1,
    )
    factor = lax.rsqrt(own_squares / D + epsilon)[:, None]
    heads_out, memory_next = head_output(
        memory_state,
        query_sum * factor,
        key_sum * factor,
        value_sum * factor,
        gate_sum * factor,
        beta_sum * factor,
        decay_sum * factor,
        decay_log,
        decay_shift,
        head_gain,
    )
    attn_rows = jnp.dot(
        collect(heads_out, "kv", 0), output_weight, preferred_element_type=jnp.float32
    )
    attn_mine = sent_and_summed_2(attn_rows, "tp", 1)
    middle = (stream.astype(jnp.float32) + attn_mine).astype(jnp.bfloat16)
    scaled_mix, squares_mix = gathered_rows(middle, mixer_gain)
    up_part = jnp.dot(scaled_mix, up_weight, preferred_element_type=jnp.float32)
    up_mine, square_mine = side_by_side(
        (up_part.astype(jnp.bfloat16), squares_mix.astype(jnp.bfloat16)), "kv", 0, 1
    )
    hidden = jnp.square(
        jax.nn.relu(up_mine * lax.rsqrt(square_mine / D + epsilon)[:, None])
    ).astype(jnp.bfloat16)
    down_rows = jnp.dot(collect(hidden, "kv", 0), down_weight, preferred_element_type=jnp.float32)
    mixer_mine = lax.psum_scatter(
        down_rows.astype(jnp.bfloat16), "tp", scatter_dimension=1, tiled=True
    ).astype(jnp.float32)
    layer_out = (middle.astype(jnp.float32) + mixer_mine).astype(jnp.bfloat16)
    return (layer_out, memory_next)


def solution(mesh):
    in_specs = (
        P(None, ("kv", "tp")),
        P("kv", "tp", None, None),
        P("kv"),
        P("kv", "tp"),
        P("kv", "tp"),
        P("kv", "tp"),
        P("kv", "tp"),
        P("kv", "tp"),
        P("kv", "tp"),
        P("tp"),
        P("tp"),
        P(),
        P("tp", "kv"),
        P("kv"),
        P("kv", "tp"),
        P("tp", "kv"),
    )
    out_specs = (P(None, ("kv", "tp")), P("kv", "tp", None, None))
    return jax.shard_map(shards, mesh=mesh, in_specs=in_specs, out_specs=out_specs, check_vma=False)
```

profile of v0, /device:TPU:8, one launch (start us, length us, event | category | flops | bytes accessed | tf_op | source)
XLA Modules:
  0.0 182.4 jit_solution(9769738742397507875)
XLA Ops:
  7.2 13.5 %all_gather.6 = bf16[128,128]{0,1:T(8,128)(2,1)S(1)} all-gather(bf16[128,16]{0,1:T(8,128)(2,1)} %param.16), channel_id=1, replica_groups=mesh['kv'=32,'tp'=8] {'tp'}, dimensions={1}, use_global_device_ids=true | all-gather | bytes 36864 | tf_op jit(solution)/shard_map/all_gather | solution.py:56
  20.8 0.9 convolution_convert_fusion.7
  21.7 0.9 convolution_convert_fusion.6
  22.6 0.1 copy.65
  22.7 0.1 copy.64
  22.8 0.2 convert_element_type.120
  23.1 1.2 convolution_convert_fusion.3
  24.3 1.2 convolution_convert_fusion.2
  25.6 0.3 convolution_convert_fusion.1
  25.9 0.3 convolution_convert_fusion.4
  26.3 2.0 %concatenate.28 = bf16[32,4,2057]{2,1,0:T(4,128)(2,1)} concatenate(bf16[32,4,512]{2,1,0:T(4,128)(2,1)S(1)} %concatenate.22, bf16[32,4,512]{2,1,0:T(4,128)(2,1)S(1)} %concatenate.23, bf16[32,4,512]{2,1,0:T(4,128)(2,1)S(1)} %concatenate.24, bf16[32,4,512]{2,1,0:T(4,128)(2,1)S(1)} %concatenate.25, bf16[32,4,4]{2,1,0:T(4,128)(2,1)S(1)} %bitcast.38, bf16[32,4,4]{2,1,0:T(4,128)(2,1)S(1)} %bitcast.37, ...), dimensions={2} | concatenate | bytes 1053184 | tf_op jit(solution)/shard_map/concatenate | solution.py:25
  28.3 11.8 %all-to-all-start = ((bf16[32,4,2057]{2,1,0:T(4,128)(2,1)}), bf16[32,4,2057]{2,1,0:T(4,128)(2,1)S(1)}, u32[]{:S(2)}, u32[]{:S(2)}) async-start(bf16[32,4,2057]{2,1,0:T(4,128)(2,1)} %concatenate.28), calls=%async_computation | async-start | bytes 1114112 | tf_op jit(solution)/shard_map/all_to_all | solution.py:19
  40.2 18.0 %all-to-all-done = bf16[32,4,2057]{2,1,0:T(4,128)(2,1)S(1)} async-done(((bf16[32,4,2057]{2,1,0:T(4,128)(2,1)}), bf16[32,4,2057]{2,1,0:T(4,128)(2,1)S(1)}, u32[]{:S(2)}, u32[]{:S(2)}) %all-to-all-start) | async-done | bytes 526624 | tf_op jit(solution)/shard_map/all_to_all | solution.py:19
  58.2 0.2 convert_reduce_fusion.1
  58.4 0.2 fusion.28
  58.6 0.1 slice_multiply_fusion.2
  58.7 0.1 multiply_reduce_fusion.1
  58.8 0.1 multiply_multiply_fusion
  58.9 0.1 multiply_reduce_fusion.2
  59.0 0.1 broadcast_multiply_fusion
  59.2 0.1 fusion.25
  59.3 0.3 fusion
  59.6 0.1 fusion.14
  59.6 0.4 multiply_add_fusion
  60.1 0.2 fusion.36
  60.3 0.1 multiply_reduce_fusion
  60.4 0.3 copy-done.11
  60.8 0.7 broadcast_in_dim.4
  61.5 5.6 %all-to-all-start.1 = ((bf16[32,4,512]{2,1,0:T(4,128)(2,1)}), bf16[32,4,512]{2,1,0:T(4,128)(2,1)S(1)}, u32[]{:S(2)}, u32[]{:S(2)}) async-start(bf16[32,4,512]{2,1,0:T(4,128)(2,1)} %broadcast_in_dim.4), calls=%async_computation.1 | async-start | bytes 262144 | tf_op jit(solution)/shard_map/all_to_all | solution.py:42
  67.1 0.1 copy.58
  67.3 8.6 %all-to-all-done.1 = bf16[32,4,512]{2,1,0:T(4,128)(2,1)S(1)} async-done(((bf16[32,4,512]{2,1,0:T(4,128)(2,1)}), bf16[32,4,512]{2,1,0:T(4,128)(2,1)S(1)}, u32[]{:S(2)}, u32[]{:S(2)}) %all-to-all-start.1) | async-done | bytes 131104 | tf_op jit(solution)/shard_map/all_to_all | solution.py:42
  75.9 0.2 convolution_bitcast_fusion
  76.1 9.1 %all_to_all.25 = f32[8,128,16]{1,2,0:T(8,128)S(1)} all-to-all(f32[8,128,16]{1,2,0:T(8,128)S(1)} %convolution_bitcast_fusion), channel_id=1, replica_groups=mesh['kv'=32,'tp'=8] {'tp'}, dimensions={0} | all-to-all | bytes 131072 | tf_op jit(solution)/shard_map/all_to_all | solution.py:51
  85.2 12.9 %all_gather.7 = bf16[128,128]{0,1:T(8,128)(2,1)S(1)} all-gather(bf16[128,16]{0,1:T(8,128)(2,1)S(1)} %add_convert_fusion.1), channel_id=1, replica_groups=mesh['kv'=32,'tp'=8] {'tp'}, dimensions={1}, use_global_device_ids=true | all-gather | bytes 36864 | tf_op jit(solution)/shard_map/all_gather | solution.py:56
  98.2 0.2 convert_element_type.121
  98.4 0.4 convolution_convert_fusion
  98.8 0.2 concatenate.29
  99.0 0.3 pad_maximum_fusion
  99.3 23.0 %all_to_all.26 = bf16[32,4,2049]{2,1,0:T(4,128)(2,1)S(1)} all-to-all(bf16[32,4,2049]{2,1,0:T(4,128)(2,1)S(1)} %pad_maximum_fusion), channel_id=1, replica_groups=mesh['kv'=32,'tp'=8] {'kv'}, dimensions={0} | all-to-all | bytes 1049088 | tf_op jit(solution)/shard_map/all_to_all | solution.py:19
  122.3 0.2 convert_reduce_fusion
  122.6 0.1 fusion.21
  122.7 0.1 fusion.10
  122.8 0.2 broadcast_in_dim.5
  123.0 21.7 %all_to_all.27 = bf16[32,4,2048]{2,1,0:T(4,128)(2,1)S(1)} all-to-all(bf16[32,4,2048]{2,1,0:T(4,128)(2,1)S(1)} %broadcast_in_dim.5), channel_id=1, replica_groups=mesh['kv'=32,'tp'=8] {'kv'}, dimensions={0} | all-to-all | bytes 1048576 | tf_op jit(solution)/shard_map/all_to_all | solution.py:42
  144.7 0.1 reshape.111
  144.9 0.9 convolution_convert_fusion.5
  145.8 28.5 %reduce-scatter.2.cloned.1.call-done = bf16[128,16]{0,1:T(8,128)(2,1)} async-done(((bf16[128,128]{0,1:T(8,128)(2,1)}), bf16[128,16]{0,1:T(8,128)(2,1)}) %reduce-scatter.2.cloned.1.call-update) | async-done | bytes 4112 | tf_op jit(solution)/shard_map/reduce_scatter | solution.py:164
  174.3 1.3 add_convert_fusion
  (46 shorter events, 0.6 us)
Async XLA Ops:
  7.2 91.3 %copy-start = (bf16[128,2048]{1,0:T(8,128)(2,1)S(1)}, bf16[128,2048]{1,0:T(8,128)(2,1)}, u32[]{:S(2)}) copy-start(bf16[128,2048]{1,0:T(8,128)(2,1)} %param.30) | copy-start | bytes 1572868
  7.2 18.4 %copy-start.8 = (f32[128]{0:T(128)S(1)}, f32[128]{0:T(128)}, u32[]{:S(2)}) copy-start(f32[128]{0:T(128)} %param.18) | copy-start | bytes 1540
  7.2 18.4 %copy-start.4 = (bf16[128,512]{1,0:T(8,128)(2,1)S(1)}, bf16[128,512]{1,0:T(8,128)(2,1)}, u32[]{:S(2)}) copy-start(bf16[128,512]{1,0:T(8,128)(2,1)} %param.22) | copy-start | bytes 393220
  7.2 18.7 %copy-start.5 = (bf16[128,512]{1,0:T(8,128)(2,1)S(1)}, bf16[128,512]{1,0:T(8,128)(2,1)}, u32[]{:S(2)}) copy-start(bf16[128,512]{1,0:T(8,128)(2,1)} %param.19) | copy-start | bytes 393220
  26.3 13.9 %copy-start.12 = (f32[4]{0:T(128)S(1)}, f32[4]{0:T(128)}, u32[]{:S(2)}) copy-start(f32[4]{0:T(128)} %param.25) | copy-start | bytes 52
  28.3 30.8 %copy-start.10 = (f32[4]{0:T(128)S(1)}, f32[4]{0:T(128)}, u32[]{:S(2)}) copy-start(f32[4]{0:T(128)} %param.26) | copy-start | bytes 52
  28.3 30.9 %copy-start.1 = (f32[4,4,128,128]{3,2,1,0:T(8,128)S(1)}, f32[4,4,128,128]{3,2,1,0:T(8,128)}, u32[]{:S(2)}) copy-start(f32[4,4,128,128]{3,2,1,0:T(8,128)} %param.17) | copy-start | bytes 3145732
  28.3 29.9 %all-to-all-start = ((bf16[32,4,2057]{2,1,0:T(4,128)(2,1)}), bf16[32,4,2057]{2,1,0:T(4,128)(2,1)S(1)}, u32[]{:S(2)}, u32[]{:S(2)}) async-start(bf16[32,4,2057]{2,1,0:T(4,128)(2,1)} %concatenate.28), calls=%async_computation | async-start | bytes 1114112 | tf_op jit(solution)/shard_map/all_to_all | solution.py:19
  60.0 16.1 %copy-start.2 = (f32[4,4,128,128]{3,2,1,0:T(8,128)}, f32[4,4,128,128]{3,2,1,0:T(8,128)S(1)}, u32[]{:S(2)}) copy-start(f32[4,4,128,128]{3,2,1,0:T(8,128)S(1)} %multiply_add_fusion) | copy-start | bytes 3145732
  60.1 0.7 copy-start.11
  60.1 7.1 %copy-start.6 = (bf16[512,128]{1,0:T(8,128)(2,1)S(1)}, bf16[512,128]{1,0:T(8,128)(2,1)}, u32[]{:S(2)}) copy-start(bf16[512,128]{1,0:T(8,128)(2,1)} %param.28) | copy-start | bytes 393220
  60.1 25.1 %copy-start.7 = (bf16[128,16]{0,1:T(8,128)(2,1)S(1)}, bf16[128,16]{0,1:T(8,128)(2,1)}, u32[]{:S(2)}) copy-start(bf16[128,16]{0,1:T(8,128)(2,1)} %param.16) | copy-start | bytes 12292
  60.3 38.1 %copy-start.9 = (f32[128]{0:T(128)S(1)}, f32[128]{0:T(128)}, u32[]{:S(2)}) copy-start(f32[128]{0:T(128)} %param.29) | copy-start | bytes 1540
  61.5 14.4 %all-to-all-start.1 = ((bf16[32,4,512]{2,1,0:T(4,128)(2,1)}), bf16[32,4,512]{2,1,0:T(4,128)(2,1)S(1)}, u32[]{:S(2)}, u32[]{:S(2)}) async-start(bf16[32,4,512]{2,1,0:T(4,128)(2,1)} %broadcast_in_dim.4), calls=%async_computation.1 | async-start | bytes 262144 | tf_op jit(solution)/shard_map/all_to_all | solution.py:42
  67.1 107.2 %reduce-scatter.2.cloned.1.call-start = ((), (), s32[]{:S(2)}) async-start(), calls=%async_computation.6 | async-start | bytes 36864 | tf_op jit(solution)/shard_map/reduce_scatter | solution.py:164
  123.0 21.8 %copy-start.3 = (bf16[2048,128]{1,0:T(8,128)(2,1)S(1)}, bf16[2048,128]{1,0:T(8,128)(2,1)}, u32[]{:S(2)}) copy-start(bf16[2048,128]{1,0:T(8,128)(2,1)} %param.31) | copy-start | bytes 1572868
Sparse Core Ops, SparseCore 0:
  145.9 28.2 reduce-scatter.1
where the time goes:
time: 183 us; the launch traced here: 182 us
  blocking collectives  80.2 us (44%)
  waiting for transfers between devices  55.1 us (30%)
  starting transfers between devices  17.4 us (10%)
  between operations  14.4 us (8%)
  matrix products  6.8 us (4%)
  local copies, waits for them, and re-layouts  4.73 us (3%)
  other arithmetic  3.69 us (2%)
    reduce_scatter x1, waiting for transfers between devices, shards(): lax.psum_scatter(down_rows.astype(jnp.bfloat16), 'tp', scatter_dimension=...  28.5 us
    all_gather x2, blocking collectives, gathered_rows(): gathered = lax.all_gather(stream, 'tp', axis=1, tiled=True)  26.4 us
    all_to_all x1, blocking collectives, sent_and_summed(): lax.all_to_all(split_up(value, dim, length), axis, 0, 0, tiled=True)  23 us
    all_to_all x1, blocking collectives, copy_for_each(): return lax.all_to_all(copies, axis, split_axis=0, concat_axis=0, tiled=True)  21.7 us
    all_to_all x1, waiting for transfers between devices, sent_and_summed(): lax.all_to_all(split_up(value, dim, length), axis, 0, 0, tiled=True)  18 us
    all_to_all x1, starting transfers between devices, sent_and_summed(): lax.all_to_all(split_up(value, dim, length), axis, 0, 0, tiled=True)  11.8 us
    all_to_all x1, blocking collectives, sent_and_summed_2(): lax.all_to_all(pieces, axis, split_axis=0, concat_axis=0, tiled=True)  9.07 us
    all_to_all x1, waiting for transfers between devices, copy_for_each(): return lax.all_to_all(copies, axis, split_axis=0, concat_axis=0, tiled=True)  8.64 us
  transfers between devices with their start and end apart: 3, of which 3 were waited for; matrix products, arithmetic and copies ran while one was open for 0% of the time, Pallas kernels for 0%

commit v1 on v0

--- a/solution.py
+++ b/solution.py
@@ -6,6 +6,14 @@
 D = 4096
 HEAD_DIM = 128
 epsilon = 1e-06
+
+
+def gather_from_all(shard, axis, dim):
+    size = lax.axis_size(axis)
+    repeats = [size if d == dim else 1 for d in range(shard.ndim)]
+    return lax.all_to_all(
+        jnp.tile(shard, repeats), axis, split_axis=dim, concat_axis=dim, tiled=True
+    )
 
 
 def split_up(value, dim, length):
@@ -53,7 +61,7 @@
 
 
 def gathered_rows(stream, gain_vec):
-    gathered = lax.all_gather(stream, "tp", axis=1, tiled=True)
+    gathered = gather_from_all(stream, "tp", 1)
     widened = gathered.astype(jnp.float32)
     squares = jnp.sum(widened * widened, axis=1)
     scaled = (widened * gain_vec).astype(jnp.bfloat16)

time: 183 us -> 172 us (0.940)
  blocking collectives: 80.2 us -> 69.1 us
    all_gather x2 -> x0, blocking collectives: 26.4 us -> none  [gathered_rows(): gathered = lax.all_gather(stream, 'tp', axis=1, tiled=True)]
    all_to_all x0 -> x2, blocking collectives: none -> 17.3 us  [gather_from_all(): lax.all_to_all(jnp.tile(shard, repeats), axis, split_axis=dim, concat_axi...]
where the time goes in v1:
time: 172 us
  blocking collectives  69.1 us (40%)
  waiting for transfers between devices  54.4 us (32%)
  starting transfers between devices  17.4 us (10%)
  between operations  14.4 us (8%)
  matrix products  6.26 us (4%)
  local copies, waits for them, and re-layouts  5.49 us (3%)
  other arithmetic  4.51 us (3%)
    reduce_scatter x1, waiting for transfers between devices, shards(): lax.psum_scatter(down_rows.astype(jnp.bfloat16), 'tp', scatter_dimension=...  28.2 us
    all_to_all x1, blocking collectives, sent_and_summed(): lax.all_to_all(split_up(value, dim, length), axis, 0, 0, tiled=True)  22.4 us
    all_to_all x1, blocking collectives, copy_for_each(): return lax.all_to_all(copies, axis, split_axis=0, concat_axis=0, tiled=True)  21.4 us
    all_to_all x1, waiting for transfers between devices, sent_and_summed(): lax.all_to_all(split_up(value, dim, length), axis, 0, 0, tiled=True)  17.4 us
    all_to_all x2, blocking collectives, gather_from_all(): lax.all_to_all(jnp.tile(shard, repeats), axis, split_axis=dim, concat_axi...  17.3 us
    all_to_all x1, starting transfers between devices, sent_and_summed(): lax.all_to_all(split_up(value, dim, length), axis, 0, 0, tiled=True)  11.8 us
    all_to_all x1, waiting for transfers between devices, copy_for_each(): return lax.all_to_all(copies, axis, split_axis=0, concat_axis=0, tiled=True)  8.73 us
    all_to_all x1, blocking collectives, sent_and_summed_2(): lax.all_to_all(pieces, axis, split_axis=0, concat_axis=0, tiled=True)  8 us
  transfers between devices with their start and end apart: 3, of which 3 were waited for; matrix products, arithmetic and copies ran while one was open for 0% of the time, Pallas kernels for 0%

profile of v1, /device:TPU:8, one launch (start us, length us, event | category | flops | bytes accessed | tf_op | source)
XLA Modules:
  0.0 171.6 jit_solution(4297507108065409718)
XLA Ops:
  7.2 0.8 tile.4
  8.0 9.5 %all_to_all.37 = bf16[128,8,16]{0,2,1:T(8,128)(2,1)S(1)} all-to-all(bf16[128,8,16]{0,2,1:T(8,128)(2,1)S(1)} %tile.4), channel_id=1, replica_groups=mesh['kv'=32,'tp'=8] {'tp'}, dimensions={1} | all-to-all | bytes 65536 | tf_op jit(solution)/shard_map/all_to_all | solution.py:14
  17.5 0.7 fusion.4
  18.2 0.8 convolution_convert_fusion.6
  19.0 0.8 convolution_convert_fusion.7
  19.9 0.1 copy.66
  20.0 0.1 copy.67
  20.2 0.2 convert_element_type.138
  20.4 1.1 convolution_convert_fusion.1
  21.6 1.1 convolution_convert_fusion.2
  22.7 0.2 convolution_convert_fusion.3
  23.0 0.2 convolution_convert_fusion.4
  23.3 2.0 %concatenate.28 = bf16[32,4,2057]{2,1,0:T(4,128)(2,1)} concatenate(bf16[32,4,512]{2,1,0:T(4,128)(2,1)S(1)} %concatenate.22, bf16[32,4,512]{2,1,0:T(4,128)(2,1)S(1)} %concatenate.23, bf16[32,4,512]{2,1,0:T(4,128)(2,1)S(1)} %concatenate.24, bf16[32,4,512]{2,1,0:T(4,128)(2,1)S(1)} %concatenate.25, bf16[32,4,4]{2,1,0:T(4,128)(2,1)S(1)} %bitcast.52, bf16[32,4,4]{2,1,0:T(4,128)(2,1)S(1)} %bitcast.53, ...), dimensions={2} | concatenate | bytes 1053184 | tf_op jit(solution)/shard_map/concatenate | solution.py:33
  25.3 11.8 %all-to-all-start.1 = ((bf16[32,4,2057]{2,1,0:T(4,128)(2,1)}), bf16[32,4,2057]{2,1,0:T(4,128)(2,1)S(1)}, u32[]{:S(2)}, u32[]{:S(2)}) async-start(bf16[32,4,2057]{2,1,0:T(4,128)(2,1)} %concatenate.28), calls=%async_computation.1 | async-start | bytes 1114112 | tf_op jit(solution)/shard_map/all_to_all | solution.py:27
  37.2 17.4 %all-to-all-done.1 = bf16[32,4,2057]{2,1,0:T(4,128)(2,1)S(1)} async-done(((bf16[32,4,2057]{2,1,0:T(4,128)(2,1)}), bf16[32,4,2057]{2,1,0:T(4,128)(2,1)S(1)}, u32[]{:S(2)}, u32[]{:S(2)}) %all-to-all-start.1) | async-done | bytes 526624 | tf_op jit(solution)/shard_map/all_to_all | solution.py:27
  54.6 0.2 convert_reduce_fusion.1
  54.9 0.2 fusion.24
  55.1 0.1 multiply_reduce_fusion.3
  55.2 0.1 multiply_multiply_fusion
  55.3 0.1 multiply_reduce_fusion.4
  55.6 0.1 fusion.21
  55.7 0.3 fusion
  56.1 0.4 multiply_add_fusion
  56.5 0.2 fusion.26
  56.8 0.1 multiply_reduce_fusion.2
  56.9 0.3 copy-done.10
  57.2 0.7 broadcast_in_dim.4
  57.9 5.6 %all-to-all-start.2 = ((bf16[32,4,512]{2,1,0:T(4,128)(2,1)}), bf16[32,4,512]{2,1,0:T(4,128)(2,1)S(1)}, u32[]{:S(2)}, u32[]{:S(2)}) async-start(bf16[32,4,512]{2,1,0:T(4,128)(2,1)} %broadcast_in_dim.4), calls=%async_computation.2 | async-start | bytes 262144 | tf_op jit(solution)/shard_map/all_to_all | solution.py:50
  63.6 0.1 copy.60
  63.7 8.7 %all-to-all-done.2 = bf16[32,4,512]{2,1,0:T(4,128)(2,1)S(1)} async-done(((bf16[32,4,512]{2,1,0:T(4,128)(2,1)}), bf16[32,4,512]{2,1,0:T(4,128)(2,1)S(1)}, u32[]{:S(2)}, u32[]{:S(2)}) %all-to-all-start.2) | async-done | bytes 131104 | tf_op jit(solution)/shard_map/all_to_all | solution.py:50
  72.5 0.2 convolution_bitcast_fusion
  72.7 8.0 %all_to_all.38 = f32[8,128,16]{1,2,0:T(8,128)S(1)} all-to-all(f32[8,128,16]{1,2,0:T(8,128)S(1)} %convolution_bitcast_fusion), channel_id=1, replica_groups=mesh['kv'=32,'tp'=8] {'tp'}, dimensions={0} | all-to-all | bytes 131072 | tf_op jit(solution)/shard_map/all_to_all | solution.py:59
  80.7 7.8 %all_to_all.39 = bf16[128,8,16]{0,2,1:T(8,128)(2,1)S(1)} all-to-all(bf16[128,8,16]{0,2,1:T(8,128)(2,1)S(1)} %tile.5), channel_id=1, replica_groups=mesh['kv'=32,'tp'=8] {'tp'}, dimensions={1} | all-to-all | bytes 65536 | tf_op jit(solution)/shard_map/all_to_all | solution.py:14
  88.6 0.2 convert_element_type.139
  88.8 0.1 fusion.3
  88.9 0.3 convolution_convert_fusion
  89.2 0.2 concatenate.29
  89.4 0.3 pad_maximum_fusion
  89.7 22.4 %all_to_all.40 = bf16[32,4,2049]{2,1,0:T(4,128)(2,1)S(1)} all-to-all(bf16[32,4,2049]{2,1,0:T(4,128)(2,1)S(1)} %pad_maximum_fusion), channel_id=1, replica_groups=mesh['kv'=32,'tp'=8] {'kv'}, dimensions={0} | all-to-all | bytes 1049088 | tf_op jit(solution)/shard_map/all_to_all | solution.py:27
  112.1 0.2 convert_reduce_fusion
  112.3 0.1 fusion.17
  112.5 0.1 fusion.7
  112.6 0.2 broadcast_in_dim.5
  112.8 21.4 %all_to_all.41 = bf16[32,4,2048]{2,1,0:T(4,128)(2,1)S(1)} all-to-all(bf16[32,4,2048]{2,1,0:T(4,128)(2,1)S(1)} %broadcast_in_dim.5), channel_id=1, replica_groups=mesh['kv'=32,'tp'=8] {'kv'}, dimensions={0} | all-to-all | bytes 1048576 | tf_op jit(solution)/shard_map/all_to_all | solution.py:50
  134.2 0.1 reshape.129
  134.3 0.9 convolution_convert_fusion.5
  135.3 28.2 %reduce-scatter.2.cloned.1.call-done = bf16[128,16]{0,1:T(8,128)(2,1)} async-done(((bf16[128,128]{0,1:T(8,128)(2,1)}), bf16[128,16]{0,1:T(8,128)(2,1)}) %reduce-scatter.2.cloned.1.call-update) | async-done | bytes 4112 | tf_op jit(solution)/shard_map/reduce_scatter | solution.py:172
  163.5 1.3 add_convert_fusion
  (48 shorter events, 0.8 us)
Async XLA Ops:
  7.2 81.7 %copy-start = (bf16[128,2048]{1,0:T(8,128)(2,1)S(1)}, bf16[128,2048]{1,0:T(8,128)(2,1)}, u32[]{:S(2)}) copy-start(bf16[128,2048]{1,0:T(8,128)(2,1)} %param.30) | copy-start | bytes 1572868
  7.2 15.6 %copy-start.4 = (bf16[128,512]{1,0:T(8,128)(2,1)S(1)}, bf16[128,512]{1,0:T(8,128)(2,1)}, u32[]{:S(2)}) copy-start(bf16[128,512]{1,0:T(8,128)(2,1)} %param.20) | copy-start | bytes 393220
  7.2 15.8 %copy-start.5 = (bf16[128,512]{1,0:T(8,128)(2,1)S(1)}, bf16[128,512]{1,0:T(8,128)(2,1)}, u32[]{:S(2)}) copy-start(bf16[128,512]{1,0:T(8,128)(2,1)} %param.19) | copy-start | bytes 393220
  23.3 13.9 %copy-start.11 = (f32[4]{0:T(128)S(1)}, f32[4]{0:T(128)}, u32[]{:S(2)}) copy-start(f32[4]{0:T(128)} %param.25) | copy-start | bytes 52
  25.3 30.3 %copy-start.9 = (f32[4]{0:T(128)S(1)}, f32[4]{0:T(128)}, u32[]{:S(2)}) copy-start(f32[4]{0:T(128)} %param.26) | copy-start | bytes 52
  25.3 30.4 %copy-start.1 = (f32[4,4,128,128]{3,2,1,0:T(8,128)S(1)}, f32[4,4,128,128]{3,2,1,0:T(8,128)}, u32[]{:S(2)}) copy-start(f32[4,4,128,128]{3,2,1,0:T(8,128)} %param.17) | copy-start | bytes 3145732
  25.3 29.3 %all-to-all-start.1 = ((bf16[32,4,2057]{2,1,0:T(4,128)(2,1)}), bf16[32,4,2057]{2,1,0:T(4,128)(2,1)S(1)}, u32[]{:S(2)}, u32[]{:S(2)}) async-start(bf16[32,4,2057]{2,1,0:T(4,128)(2,1)} %concatenate.28), calls=%async_computation.1 | async-start | bytes 1114112 | tf_op jit(solution)/shard_map/all_to_all | solution.py:27
  56.5 16.2 %copy-start.2 = (f32[4,4,128,128]{3,2,1,0:T(8,128)}, f32[4,4,128,128]{3,2,1,0:T(8,128)S(1)}, u32[]{:S(2)}) copy-start(f32[4,4,128,128]{3,2,1,0:T(8,128)S(1)} %multiply_add_fusion) | copy-start | bytes 3145732
  56.5 0.7 copy-start.10
  56.5 7.1 %copy-start.6 = (bf16[512,128]{1,0:T(8,128)(2,1)S(1)}, bf16[512,128]{1,0:T(8,128)(2,1)}, u32[]{:S(2)}) copy-start(bf16[512,128]{1,0:T(8,128)(2,1)} %param.28) | copy-start | bytes 393220
  56.5 24.2 %copy-start.7 = (bf16[128,16]{0,1:T(8,128)(2,1)S(1)}, bf16[128,16]{0,1:T(8,128)(2,1)}, u32[]{:S(2)}) copy-start(bf16[128,16]{0,1:T(8,128)(2,1)} %param.16) | copy-start | bytes 12292
  56.8 32.0 %copy-start.8 = (f32[128]{0:T(128)S(1)}, f32[128]{0:T(128)}, u32[]{:S(2)}) copy-start(f32[128]{0:T(128)} %param.29) | copy-start | bytes 1540
  57.9 14.5 %all-to-all-start.2 = ((bf16[32,4,512]{2,1,0:T(4,128)(2,1)}), bf16[32,4,512]{2,1,0:T(4,128)(2,1)S(1)}, u32[]{:S(2)}, u32[]{:S(2)}) async-start(bf16[32,4,512]{2,1,0:T(4,128)(2,1)} %broadcast_in_dim.4), calls=%async_computation.2 | async-start | bytes 262144 | tf_op jit(solution)/shard_map/all_to_all | solution.py:50
  63.5 100.0 %reduce-scatter.2.cloned.1.call-start = ((), (), s32[]{:S(2)}) async-start(), calls=%async_computation.8 | async-start | bytes 36864 | tf_op jit(solution)/shard_map/reduce_scatter | solution.py:172
  112.8 21.5 %copy-start.3 = (bf16[2048,128]{1,0:T(8,128)(2,1)S(1)}, bf16[2048,128]{1,0:T(8,128)(2,1)}, u32[]{:S(2)}) copy-start(bf16[2048,128]{1,0:T(8,128)(2,1)} %param.31) | copy-start | bytes 1572868
Sparse Core Ops, SparseCore 0:
  135.4 28.0 reduce-scatter.1
